TPU v7x, 32 devices: a whole 2x2x4 slice. The times are simulated.
32 devices in a mesh: sp: 8 (over z, y), tp: 4 (over x, core).
Axes of the slice: x: 2, y: 2, z: 4, core: 2. Of those that a mesh axis runs over, the one named last changes fastest.
Arguments:
- tokens: bfloat16 [2048, 2048], P(('sp', 'tp')), may hold values from -16 to 16
- w_query: bfloat16 [2048, 1024], P(None, 'tp'), may hold values from -1 to 1
- w_key: bfloat16 [2048, 256], P(None, 'tp'), may hold values from -1 to 1
- w_value: bfloat16 [2048, 256], P(None, 'tp'), may hold values from -0.125 to 0.125
- w_gate: bfloat16 [2048, 16], P(None, 'tp'), may hold values from -0.125 to 0.125
- gate_bias: float32 [16], P('tp'), as said below
- w_output: bfloat16 [1024, 2048], P('tp'), may hold values from -0.1875 to 0.1875
Outputs:
- mixed: bfloat16 [2048, 2048], P(('sp', 'tp'))
Inputs may be any that keep to these rules, and one draw needn't show every extreme that they name: `gate_bias`: each head's forget gate bias is 4 or more; there is no upper bound.
All inputs are finite; a program needn't handle non-finite values.
Results may differ from a plain program's by a relative error of at most 0.012.
The roundings to bfloat16 on the way count: a program that leaves them out, or rounds other values in their place, can miss the bound.
Values may be sent and summed in bfloat16 or wider, within the bound.
A program may use at most 64 MiB of HBM per device.

v0:
```python
import math
import jax
import jax.numpy as jnp
from jax import lax
from jax.sharding import PartitionSpec as P

HEAD = 64
masked_value = -1e30


def softmax_update(
    carry_state,
    query_here,
    query_cumul,
    query_position,
    key_here,
    value_here,
    key_cumul,
    key_position,
):
    row_peak, row_mass, row_accum = carry_state
    scores = jnp.einsum(
        "kgtd,skd->kgts", query_here, key_here, preferred_element_type=jnp.float32
    ) * HEAD ** (-0.5)
    scores = scores + query_cumul[:, :, :, None] - key_cumul[:, :, None, :]
    allowed = key_position[None, :] <= query_position[:, None]
    scores = jnp.where(allowed, scores, masked_value)
    new_peak = jnp.maximum(row_peak, jnp.max(scores, axis=3))
    weights = jnp.where(allowed, jnp.exp(scores - new_peak[:, :, :, None]), 0.0)
    rescale = jnp.exp(row_peak - new_peak)
    row_mass = row_mass * rescale + jnp.sum(weights, axis=3)
    row_accum = row_accum * rescale[:, :, :, None] + jnp.einsum(
        "kgts,skd->kgtd",
        weights.astype(jnp.bfloat16),
        value_here,
        preferred_element_type=jnp.float32,
    )
    return (new_peak, row_mass, row_accum)


def shards(tokens, w_query, w_key, w_value, w_gate, gate_bias, w_output):
    sp_count = lax.axis_size("sp")
    sp_rank = lax.axis_index("sp")
    query_cols = w_query.shape[1]
    key_cols = w_key.shape[1]
    heads_here = w_gate.shape[1]
    kv_heads_here = key_cols // HEAD
    group_size = heads_here // kv_heads_here
    joined = jnp.concatenate([w_query, w_key, w_value, w_gate], axis=1)
    projected = jnp.dot(
        lax.all_gather(tokens, "tp", axis=0, tiled=True), joined, preferred_element_type=jnp.float32
    ).astype(jnp.bfloat16)
    local_rows = projected.shape[0]
    half_rows = local_rows // 2
    second_block = 2 * sp_rank + 1
    own_gates = jax.nn.log_sigmoid(
        projected[:, query_cols + 2 * key_cols :].astype(jnp.float32) + gate_bias
    )
    totals = jnp.sum(own_gates.reshape(2, half_rows, heads_here), axis=1)
    all_totals = lax.all_gather(totals[None], "sp", axis=0, tiled=True)
    ordered = all_totals.reshape(2 * sp_count, heads_here)
    prefix_sums = jnp.cumsum(ordered, axis=0) - ordered
    queries = (
        projected[:, :query_cols]
        .reshape(2, half_rows, kv_heads_here, group_size, HEAD)
        .transpose(0, 2, 3, 1, 4)
    )
    query_blocks = (2 * sp_rank, second_block)
    query_cumul = []
    query_position = []
    for side_index in range(2):
        base_value = lax.dynamic_index_in_dim(
            prefix_sums, query_blocks[side_index], 0, keepdims=False
        )
        cumul_rows = base_value[None, :] + jnp.cumsum(
            own_gates[side_index * half_rows : (side_index + 1) * half_rows], axis=0
        )
        query_cumul.append(
            cumul_rows.reshape(half_rows, kv_heads_here, group_size).transpose(1, 2, 0)
        )
        query_position.append(
            query_blocks[side_index] * half_rows + jnp.arange(half_rows, dtype=jnp.int32)
        )
    initial = (
        jnp.full((2, kv_heads_here, group_size, half_rows), masked_value, jnp.float32),
        jnp.zeros((2, kv_heads_here, group_size, half_rows), jnp.float32),
        jnp.zeros((2, kv_heads_here, group_size, half_rows, HEAD), jnp.float32),
    )
    gathered = lax.all_gather(projected[:, query_cols:], "sp", axis=0, tiled=True)
    row_count = gathered.shape[0]
    piece_blocks = row_count // half_rows
    per_step = math.gcd(piece_blocks, max(1, 1024 // half_rows))
    step_rows = per_step * half_rows
    step_count = row_count // step_rows
    first_row = half_rows * jnp.arange(piece_blocks, dtype=jnp.int32)
    owner_rank = first_row // local_rows
    half_index = first_row % local_rows // half_rows
    block_ids = 2 * owner_rank + half_index
    gate_logs = jax.nn.log_sigmoid(gathered[:, 2 * key_cols :].astype(jnp.float32) + gate_bias)
    gate_logs = gate_logs.reshape(piece_blocks, half_rows, heads_here)
    base_values = jnp.take(prefix_sums, block_ids, axis=0)
    key_cumul_all = (base_values[:, None, :] + jnp.cumsum(gate_logs, axis=1)).reshape(
        row_count, kv_heads_here, group_size
    )
    key_position_all = (
        block_ids[:, None] * half_rows + jnp.arange(half_rows, dtype=jnp.int32)[None, :]
    ).reshape(row_count)
    earliest = jnp.min(block_ids.reshape(step_count, per_step), axis=1)

    def one_step(step_index, inner_state):
        start_row = step_index * step_rows
        block_rows = lax.dynamic_slice_in_dim(gathered, start_row, step_rows, 0)
        key_here = block_rows[:, :key_cols].reshape(step_rows, kv_heads_here, HEAD)
        value_here = block_rows[:, key_cols : 2 * key_cols].reshape(step_rows, kv_heads_here, HEAD)
        key_cumul = lax.dynamic_slice_in_dim(key_cumul_all, start_row, step_rows, 0).transpose(
            1, 2, 0
        )
        key_position = lax.dynamic_slice_in_dim(key_position_all, start_row, step_rows, 0)
        first_id = earliest[step_index]
        results = []
        for side_index in range(2):
            head_state = tuple((member[side_index] for member in inner_state))

            def compute(head_state, side_index=side_index):
                return softmax_update(
                    head_state,
                    queries[side_index],
                    query_cumul[side_index],
                    query_position[side_index],
                    key_here,
                    value_here,
                    key_cumul,
                    key_position,
                )

            head_state = lax.cond(
                first_id <= query_blocks[side_index],
                compute,
                lambda unchanged: unchanged,
                head_state,
            )
            results.append(head_state)
        return tuple((jnp.stack([results[0][member], results[1][member]]) for member in range(3)))

    row_peak, row_mass, row_accum = lax.fori_loop(0, step_count, one_step, initial)
    attended = (row_accum / row_mass[:, :, :, :, None]).astype(jnp.bfloat16)
    attended = attended.transpose(0, 3, 1, 2, 4).reshape(local_rows, heads_here * HEAD)
    return lax.psum_scatter(
        jnp.dot(attended, w_output, preferred_element_type=jnp.float32).astype(jnp.bfloat16),
        "tp",
        scatter_dimension=0,
        tiled=True,
    )


def solution(mesh):
    return jax.shard_map(
        shards,
        mesh=mesh,
        in_specs=(
            P(("sp", "tp"), None),
            P(None, "tp"),
            P(None, "tp"),
            P(None, "tp"),
            P(None, "tp"),
            P("tp"),
            P("tp", None),
        ),
        out_specs=P(("sp", "tp"), None),
        check_vma=False,
    )
```

profile of v0, /device:TPU:0, one launch (start us, length us, event | category | flops | bytes accessed | tf_op | source)
XLA Modules:
  0.0 130.7 jit_solution(12914409057158961123)
XLA Ops:
  6.5 0.0 copy-start
  6.5 0.0 all-gather.4.cloned.1.call-start
  6.5 0.7 all-gather.4.cloned.1.call-update
  7.3 0.0 reduce-scatter.2.cloned.1.call-start
  7.3 1.0 copy.42
  8.3 1.2 copy.41
  9.6 1.2 copy.40
  10.8 0.1 add_reduce_fusion
  11.0 0.1 add_bitcast_fusion.2
  11.1 0.0 copy-start.1
  11.1 17.2 %all-gather.4.cloned.1.call-done = bf16[256,2048]{1,0:T(8,128)(2,1)} async-done(((bf16[64,2048]{1,0:T(8,128)(2,1)}), bf16[256,2048]{1,0:T(8,128)(2,1)}) %all-gather.4.cloned.1.call-update) | async-done | bytes 1048592 | tf_op jit(solution)/shard_map/all_gather | solution.py:51
  28.3 2.7 %fusion.47 = bf16[256,388]{0,1:T(8,128)(2,1)S(1)} fusion(bf16[256,2048]{1,0:T(8,128)(2,1)} %all-gather.4.cloned.1.call-done, bf16[2048,4]{1,0:T(8,128)(2,1)S(1)} %copy.42, bf16[2048,64]{1,0:T(8,128)(2,1)S(1)} %copy.41, bf16[2048,64]{1,0:T(8,128)(2,1)S(1)} %copy.40, bf16[2048,256]{1,0:T(8,128)(2,1)} %param.14), kind=kOutput, calls=%fused_computation.71 | convolution fusion | flops 413303808 | bytes 2836480 | tf_op jit(solution)/shard_map/dot_general | solution.py:50
  31.1 0.0 copy-done.1
  31.1 0.1 fusion.55
  31.2 31.5 %all_gather.10 = bf16[2048,132]{0,1:T(8,128)(2,1)S(1)} all-gather(bf16[256,132]{0,1:T(8,128)(2,1)S(1)} %slice.96), channel_id=1, replica_groups=mesh['sp'=8,'tp'=4] {'sp'}, dimensions={0}, use_global_device_ids=true | all-gather | bytes 608256 | tf_op jit(solution)/shard_map/all_gather | solution.py:89
  62.8 0.1 reduce_sum.31
  62.8 0.1 copy.43
  62.9 20.5 %all-gather.1 = f32[8,2,4]{2,1,0:T(2,128)S(1)} all-gather(f32[1,2,4]{2,1,0:T(2,128)S(1)} %bitcast.194), channel_id=2, replica_groups=mesh['sp'=8,'tp'=4] {'sp'}, dimensions={0}, use_global_device_ids=true | all-gather | bytes 288 | tf_op jit(solution)/shard_map/all_gather | solution.py:60
  83.4 0.1 fusion.54
  83.6 0.5 copy.44
  84.1 0.6 gather_fusion
  84.7 0.1 broadcast_select_fusion
  84.8 1.2 broadcast_add_fusion.2
  85.9 1.6 %copy.45 = f32[16,128,4]{1,0,2:T(8,128)S(1)} copy(f32[16,128,4]{2,0,1:T(8,128)} %broadcast_add_fusion.2) | data formatting | bytes 65536 | tf_op jit(solution)/shard_map/add | solution.py:102
  87.6 0.1 copy.48
  87.7 0.1 fusion.62
  87.9 0.1 copy.47
  88.0 0.1 fusion.61
  88.1 0.1 add_bitcast_fusion
  88.2 0.1 copy.49
  88.3 0.1 copy.50
  88.4 9.0 %while.18 = (s32[]{:T(128)}, f32[2,1,4,128]{3,2,1,0:T(4,128)S(1)}, f32[2,1,4,128]{3,2,1,0:T(4,128)S(1)}, f32[2,1,4,128,64]{3,4,2,1,0:T(8,128)S(1)}, s32[2]{0:T(1...) while((s32[]{:T(128)}, f32[2,1,4,128]{3,2,1,0:T(4,128)S(1)}, ...), condition=%wide.region_15.16_spmd.clone, body=%wide.region_6.15_spmd.clone.sunk | while | flops 280433920 | bytes 16568903 | solution.py:145
  88.4 0.7 dynamic_slice.54
  89.9 2.2 %conditional.6 = (f32[1,1,4,128]{3,2,1,0:T(4,128)S(1)}, f32[1,1,4,128]{3,2,1,0:T(4,128)S(1)}, f32[1,1,4,128,64]{3,4,2,1,0:T(8,128)S(1)}) conditional(s32[]{:T(128)} %convert_element_type.63, (f32[1,4,128]{2,1,0:T(4,128)S(1)}, f32[1,4,128]{2,1,0:T(4,128)S(1)}, f32[1,4,128,64]{2,3,1,0:T(8,128)S(1)}) %tuple.137, (s32[1024]{0:T(1024)S(1)}, s32[]{:T(128)}, ...), branch_computations={%region_11.11_spmd, %region_12.14_spmd} | conditional | flops 140183168 | bytes 7460380 | solution.py:136
  90.0 0.1 broadcast_compare_fusion.1
  90.1 0.8 fusion.60
  90.9 0.6 fusion.21
  91.5 0.6 fusion.23
  92.8 2.2 %conditional.7 = (f32[1,1,4,128]{3,2,1,0:T(4,128)S(1)}, f32[1,1,4,128]{3,2,1,0:T(4,128)S(1)}, f32[1,1,4,128,64]{3,4,2,1,0:T(8,128)S(1)}) conditional(s32[]{:T(128)} %convert_element_type.64, (f32[1,4,128]{2,1,0:T(4,128)S(1)}, f32[1,4,128]{2,1,0:T(4,128)S(1)}, f32[1,4,128,64]{2,3,1,0:T(8,128)S(1)}) %tuple.139, (s32[1024]{0:T(1024)S(1)}, s32[]{:T(128)}, ...), branch_computations={%region_7.7_spmd, %region_8.10_spmd} | conditional | flops 140183168 | bytes 7460380 | solution.py:136
  92.9 0.1 broadcast_compare_fusion
  93.0 0.8 fusion.59
  93.8 0.6 fusion.5
  94.4 0.6 fusion.7
  95.1 0.7 dynamic_slice.54
  97.4 0.1 copy.51
  97.6 0.0 copy-done
  97.6 1.5 %convolution_convert_fusion = bf16[256,2048]{1,0:T(8,128)(2,1)} fusion(bf16[256,2048]{1,0:T(8,128)(2,1)S(1)} %copy-done, bf16[32,8,2,128]{3,2,1,0:T(2,128)(2,1)S(1)} %bitcast.184), kind=kOutput, calls=%fused_computation.61 | convolution fusion | flops 268959744 | bytes 2228224 | tf_op jit(solution)/shard_map/dot_general | solution.py:149
  99.0 0.0 reduce-scatter.2.cloned.1.call-update
  99.1 24.8 %reduce-scatter.2.cloned.1.call-done = bf16[64,2048]{1,0:T(8,128)(2,1)} async-done(((bf16[256,2048]{1,0:T(8,128)(2,1)}), bf16[64,2048]{1,0:T(8,128)(2,1)}) %reduce-scatter.2.cloned.1.call-update) | async-done | bytes 262160 | tf_op jit(solution)/shard_map/reduce_scatter | solution.py:148
  (47 shorter events, 0.6 us)
Async XLA Ops:
  6.5 91.0 %copy-start = (bf16[256,2048]{1,0:T(8,128)(2,1)S(1)}, bf16[256,2048]{1,0:T(8,128)(2,1)}, u32[]{:S(2)}) copy-start(bf16[256,2048]{1,0:T(8,128)(2,1)} %param.19) | copy-start | bytes 3145732
  6.5 21.8 %all-gather.4.cloned.1.call-start = ((), (), s32[]{:S(2)}) async-start(), calls=%async_computation.1 | async-start | bytes 1310720 | tf_op jit(solution)/shard_map/all_gather | solution.py:51
  7.3 116.6 %reduce-scatter.2.cloned.1.call-start = ((), (), s32[]{:S(2)}) async-start(), calls=%async_computation.2 | async-start | bytes 1310720 | tf_op jit(solution)/shard_map/reduce_scatter | solution.py:148
  11.1 20.0 %copy-start.1 = (f32[4]{0:T(128)S(1)}, f32[4]{0:T(128)}, u32[]{:S(2)}) copy-start(f32[4]{0:T(128)} %param.18) | copy-start | bytes 52
Sparse Core Ops, SparseCore 0:
  8.9 19.4 all-gather.3
  99.2 24.6 reduce-scatter.1
where the time goes:
time: 131 us
  blocking collectives  52 us (40%)
  waiting for transfers between devices  42.8 us (33%)
  between operations  13.6 us (10%)
  local copies, waits for them, and re-layouts  8.46 us (6%)
  matrix products  6.94 us (5%)
  other arithmetic  3.82 us (3%)
  loops' own time  3.1 us (2%)
    all_gather x1, blocking collectives, shards(): lax.all_gather(projected[:, query_cols:], 'sp', axis=0, tiled=True)  31.5 us
    reduce_scatter x1, waiting for transfers between devices, shards(): lax.psum_scatter(jnp.dot(attended, w_output, preferred_element_type=jnp.f...  24.8 us
    all_gather x1, blocking collectives, shards(): all_totals = lax.all_gather(totals[None], 'sp', axis=0, tiled=True)  20.5 us
    all_gather x1, waiting for transfers between devices, shards(): lax.all_gather(tokens, 'tp', axis=0, tiled=True)  17.2 us
    unnamed x10, local copies, waits for them, and re-layouts  3.63 us
    another operation x1, loops' own time, shards(): lax.fori_loop(0, step_count, one_step, initial)  3.01 us
    dot_general x1, matrix products, shards(): jnp.dot(lax.all_gather(tokens, 'tp', axis=0, tiled=True), joined, preferr...  2.72 us
  transfers between devices with their start and end apart: 2, of which 2 were waited for; matrix products, arithmetic and copies ran while one was open for 3% of the time, Pallas kernels for 0%

commit v1 on v0

--- a/solution.py
+++ b/solution.py
@@ -48,7 +48,11 @@
     group_size = heads_here // kv_heads_here
     joined = jnp.concatenate([w_query, w_key, w_value, w_gate], axis=1)
     projected = jnp.dot(
-        lax.all_gather(tokens, "tp", axis=0, tiled=True), joined, preferred_element_type=jnp.float32
+        jnp.concatenate(
+            lax.all_to_all(jnp.stack([tokens] * lax.axis_size("tp")), "tp", 0, 0), axis=0
+        ),
+        joined,
+        preferred_element_type=jnp.float32,
     ).astype(jnp.bfloat16)
     local_rows = projected.shape[0]
     half_rows = local_rows // 2

time: 131 us -> 131 us (level)
  waiting for transfers between devices: 42.8 us -> 36.4 us
  starting transfers between devices: 0.04 us -> 4.24 us
    all_gather x1 -> x0, waiting for transfers between devices: 17.2 us -> none  [shards(): lax.all_gather(tokens, 'tp', axis=0, tiled=True)]
    all_to_all x0 -> x1, waiting for transfers between devices: none -> 11.5 us  [shards(): lax.all_to_all(jnp.stack([tokens] * lax.axis_size('tp')), 'tp', 0, 0)]
    all_to_all x0 -> x1, starting transfers between devices: none -> 4.24 us  [shards(): lax.all_to_all(jnp.stack([tokens] * lax.axis_size('tp')), 'tp', 0, 0)]
    another operation x0 -> x1, local copies, waits for them, and re-layouts: none -> 2.16 us  [shards(): jnp.stack([tokens] * lax.axis_size('tp'))]
    unnamed x10 -> x14, local copies, waits for them, and re-layouts: 3.63 us -> 2.73 us
  transfers between devices with their start and end apart: 2 -> 2, of which waited for: 2 -> 2; matrix products, arithmetic and copies ran while one was open for 3% -> 2% of each run, Pallas kernels for 0% -> 0%
where the time goes in v1:
time: 131 us
  blocking collectives  53.1 us (41%)
  waiting for transfers between devices  36.4 us (28%)
  between operations  13.6 us (10%)
  local copies, waits for them, and re-layouts  9.72 us (7%)
  matrix products  6.76 us (5%)
  starting transfers between devices  4.24 us (3%)
  other arithmetic  3.82 us (3%)
  loops' own time  3.1 us (2%)
    all_gather x1, blocking collectives, shards(): lax.all_gather(projected[:, query_cols:], 'sp', axis=0, tiled=True)  32.8 us
    reduce_scatter x1, waiting for transfers between devices, shards(): lax.psum_scatter(jnp.dot(attended, w_output, preferred_element_type=jnp.f...  24.8 us
    all_gather x1, blocking collectives, shards(): all_totals = lax.all_gather(totals[None], 'sp', axis=0, tiled=True)  20.3 us
    all_to_all x1, waiting for transfers between devices, shards(): lax.all_to_all(jnp.stack([tokens] * lax.axis_size('tp')), 'tp', 0, 0)  11.5 us
    all_to_all x1, starting transfers between devices, shards(): lax.all_to_all(jnp.stack([tokens] * lax.axis_size('tp')), 'tp', 0, 0)  4.24 us
    another operation x1, loops' own time, shards(): lax.fori_loop(0, step_count, one_step, initial)  3.01 us
    unnamed x14, local copies, waits for them, and re-layouts  2.73 us
  transfers between devices with their start and end apart: 2, of which 2 were waited for; matrix products, arithmetic and copies ran while one was open for 2% of the time, Pallas kernels for 0%

profile of v1, /device:TPU:0, one launch (start us, length us, event | category | flops | bytes accessed | tf_op | source)
XLA Modules:
  0.0 130.7 jit_solution(212295692415183427)
XLA Ops:
  6.5 0.0 copy-start
  6.5 0.0 copy-start.2
  6.5 0.0 copy-start.1
  6.5 2.2 %stack.106 = bf16[4,64,2048]{2,1,0:T(8,128)(2,1)} broadcast(bf16[64,2048]{1,0:T(8,128)(2,1)} %param.13), dimensions={1,2} | broadcast | bytes 1310720 | tf_op jit(solution)/shard_map/stack | solution.py:52
  8.7 4.2 %all-to-all-start = ((bf16[4,64,2048]{2,1,0:T(8,128)(2,1)}), bf16[4,64,2048]{2,1,0:T(8,128)(2,1)S(1)}, u32[]{:S(2)}, u32[]{:S(2)}) async-start(bf16[4,64,2048]{2,1,0:T(8,128)(2,1)} %stack.106), calls=%async_computation | async-start | bytes 2097152 | tf_op jit(solution)/shard_map/all_to_all | solution.py:52
  12.9 0.0 reduce-scatter.2.cloned.1.call-start
  12.9 0.0 copy-done.2
  12.9 1.1 copy.42
  14.0 0.0 copy-done.1
  14.0 0.3 copy.41
  14.3 1.2 copy.40
  15.5 0.1 add_reduce_fusion
  15.8 0.1 add_bitcast_fusion.2
  15.8 11.5 %all-to-all-done = bf16[4,64,2048]{2,1,0:T(8,128)(2,1)S(1)} async-done(((bf16[4,64,2048]{2,1,0:T(8,128)(2,1)}), bf16[4,64,2048]{2,1,0:T(8,128)(2,1)S(1)}, u32[]{:S(2)}, u32[]{:S(2)}) %all-to-all-start) | async-done | bytes 1048608 | tf_op jit(solution)/shard_map/all_to_all | solution.py:52
  27.4 0.0 copy-start.3
  27.4 2.5 %fusion.47 = bf16[256,388]{0,1:T(8,128)(2,1)S(1)} fusion(bf16[256,2048]{1,0:T(8,128)(2,1)S(1)} %bitcast.183, bf16[2048,4]{1,0:T(8,128)(2,1)} %copy.42, bf16[2048,64]{1,0:T(8,128)(2,1)S(1)} %copy.41, bf16[2048,64]{1,0:T(8,128)(2,1)S(1)} %copy.40, bf16[2048,256]{1,0:T(8,128)(2,1)} %param.14), kind=kOutput, calls=%fused_computation.71 | convolution fusion | flops 413303808 | bytes 2836480 | tf_op jit(solution)/shard_map/dot_general | solution.py:50
  29.9 0.0 copy-done.3
  30.0 0.1 fusion.55
  30.1 32.8 %all_gather.6 = bf16[2048,132]{0,1:T(8,128)(2,1)S(1)} all-gather(bf16[256,132]{0,1:T(8,128)(2,1)S(1)} %slice.96), channel_id=1, replica_groups=mesh['sp'=8,'tp'=4] {'sp'}, dimensions={0}, use_global_device_ids=true | all-gather | bytes 608256 | tf_op jit(solution)/shard_map/all_gather | solution.py:93
  62.8 0.1 reduce_sum.31
  62.9 0.1 copy.43
  63.0 20.3 %all-gather.1 = f32[8,2,4]{2,1,0:T(2,128)S(1)} all-gather(f32[1,2,4]{2,1,0:T(2,128)S(1)} %bitcast.196), channel_id=2, replica_groups=mesh['sp'=8,'tp'=4] {'sp'}, dimensions={0}, use_global_device_ids=true | all-gather | bytes 288 | tf_op jit(solution)/shard_map/all_gather | solution.py:64
  83.4 0.1 fusion.54
  83.5 0.5 copy.44
  84.0 0.6 gather_fusion
  84.6 0.1 broadcast_select_fusion
  84.7 1.2 broadcast_add_fusion.2
  85.8 1.6 %copy.45 = f32[16,128,4]{1,0,2:T(8,128)S(1)} copy(f32[16,128,4]{2,0,1:T(8,128)} %broadcast_add_fusion.2) | data formatting | bytes 65536 | tf_op jit(solution)/shard_map/add | solution.py:106
  87.5 0.1 copy.48
  87.7 0.1 fusion.62
  87.8 0.1 copy.47
  87.9 0.1 fusion.61
  88.1 0.1 add_bitcast_fusion
  88.2 0.1 copy.49
  88.2 0.1 copy.50
  88.3 9.0 %while.18 = (s32[]{:T(128)}, f32[2,1,4,128]{3,2,1,0:T(4,128)S(1)}, f32[2,1,4,128]{3,2,1,0:T(4,128)S(1)}, f32[2,1,4,128,64]{3,4,2,1,0:T(8,128)S(1)}, s32[2]{0:T(1...) while((s32[]{:T(128)}, f32[2,1,4,128]{3,2,1,0:T(4,128)S(1)}, ...), condition=%wide.region_15.16_spmd.clone, body=%wide.region_6.15_spmd.clone.sunk | while | flops 280433920 | bytes 16568903 | solution.py:149
  88.4 0.7 dynamic_slice.54
  89.8 2.2 %conditional.6 = (f32[1,1,4,128]{3,2,1,0:T(4,128)S(1)}, f32[1,1,4,128]{3,2,1,0:T(4,128)S(1)}, f32[1,1,4,128,64]{3,4,2,1,0:T(8,128)S(1)}) conditional(s32[]{:T(128)} %convert_element_type.63, (f32[1,4,128]{2,1,0:T(4,128)S(1)}, f32[1,4,128]{2,1,0:T(4,128)S(1)}, f32[1,4,128,64]{2,3,1,0:T(8,128)S(1)}) %tuple.137, (s32[1024]{0:T(1024)S(1)}, s32[]{:T(128)}, ...), branch_computations={%region_11.11_spmd, %region_12.14_spmd} | conditional | flops 140183168 | bytes 7460380 | solution.py:140
  89.9 0.1 broadcast_compare_fusion.1
  90.0 0.8 fusion.60
  90.8 0.6 fusion.21
  91.4 0.6 fusion.23
  92.7 2.2 %conditional.7 = (f32[1,1,4,128]{3,2,1,0:T(4,128)S(1)}, f32[1,1,4,128]{3,2,1,0:T(4,128)S(1)}, f32[1,1,4,128,64]{3,4,2,1,0:T(8,128)S(1)}) conditional(s32[]{:T(128)} %convert_element_type.64, (f32[1,4,128]{2,1,0:T(4,128)S(1)}, f32[1,4,128]{2,1,0:T(4,128)S(1)}, f32[1,4,128,64]{2,3,1,0:T(8,128)S(1)}) %tuple.139, (s32[1024]{0:T(1024)S(1)}, s32[]{:T(128)}, ...), branch_computations={%region_7.7_spmd, %region_8.10_spmd} | conditional | flops 140183168 | bytes 7460380 | solution.py:140
  92.8 0.1 broadcast_compare_fusion
  92.9 0.8 fusion.59
  93.7 0.6 fusion.5
  94.3 0.6 fusion.7
  95.0 0.7 dynamic_slice.54
  97.3 0.1 copy.51
  97.5 0.0 copy-done
  97.5 1.5 %convolution_convert_fusion = bf16[256,2048]{1,0:T(8,128)(2,1)} fusion(bf16[256,2048]{1,0:T(8,128)(2,1)S(1)} %copy-done, bf16[32,8,2,128]{3,2,1,0:T(2,128)(2,1)S(1)} %bitcast.186), kind=kOutput, calls=%fused_computation.61 | convolution fusion | flops 268959744 | bytes 2228224 | tf_op jit(solution)/shard_map/dot_general | solution.py:153
  98.9 0.0 reduce-scatter.2.cloned.1.call-update
  99.0 24.8 %reduce-scatter.2.cloned.1.call-done = bf16[64,2048]{1,0:T(8,128)(2,1)} async-done(((bf16[256,2048]{1,0:T(8,128)(2,1)}), bf16[64,2048]{1,0:T(8,128)(2,1)}) %reduce-scatter.2.cloned.1.call-update) | async-done | bytes 262160 | tf_op jit(solution)/shard_map/reduce_scatter | solution.py:152
  (47 shorter events, 0.6 us)
Async XLA Ops:
  6.5 91.0 %copy-start = (bf16[256,2048]{1,0:T(8,128)(2,1)S(1)}, bf16[256,2048]{1,0:T(8,128)(2,1)}, u32[]{:S(2)}) copy-start(bf16[256,2048]{1,0:T(8,128)(2,1)} %param.19) | copy-start | bytes 3145732
  6.5 6.4 %copy-start.2 = (bf16[2048,4]{0,1:T(4,128)(2,1)S(1)}, bf16[2048,4]{0,1:T(4,128)(2,1)}, u32[]{:S(2)}) copy-start(bf16[2048,4]{0,1:T(4,128)(2,1)} %param.17) | copy-start | bytes 49156
  6.5 7.5 %copy-start.1 = (bf16[2048,64]{0,1:T(8,128)(2,1)S(1)}, bf16[2048,64]{0,1:T(8,128)(2,1)}, u32[]{:S(2)}) copy-start(bf16[2048,64]{0,1:T(8,128)(2,1)} %param.16) | copy-start | bytes 786436
  8.7 18.7 %all-to-all-start = ((bf16[4,64,2048]{2,1,0:T(8,128)(2,1)}), bf16[4,64,2048]{2,1,0:T(8,128)(2,1)S(1)}, u32[]{:S(2)}, u32[]{:S(2)}) async-start(bf16[4,64,2048]{2,1,0:T(8,128)(2,1)} %stack.106), calls=%async_computation | async-start | bytes 2097152 | tf_op jit(solution)/shard_map/all_to_all | solution.py:52
  12.9 110.9 %reduce-scatter.2.cloned.1.call-start = ((), (), s32[]{:S(2)}) async-start(), calls=%async_computation.2 | async-start | bytes 1310720 | tf_op jit(solution)/shard_map/reduce_scatter | solution.py:152
  27.4 2.6 %copy-start.3 = (f32[4]{0:T(128)S(1)}, f32[4]{0:T(128)}, u32[]{:S(2)}) copy-start(f32[4]{0:T(128)} %param.18) | copy-start | bytes 52
Sparse Core Ops, SparseCore 0:
  99.1 24.6 reduce-scatter.1
